TPU v7x, 32 devices: a whole 2x2x4 slice. The times are simulated.
32 devices in a mesh: ep: 4 (over y, x), tp: 8 (over z, core).
Axes of the slice: x: 2, y: 2, z: 4, core: 2. Of those that a mesh axis runs over, the one named last changes fastest.
Arguments:
- tokens: bfloat16 [1024, 4096], P('ep'), may hold values from -6 to 6
- cotangent: bfloat16 [1024, 4096], P('ep'), may hold values from -6 to 6
- routing: int32 [1024, 2], P('ep'), may hold values from 0 to 3, all different within a row; in each aligned block of 256 rows (0 to 255, 256 to 511, ...) at most 160 rows name the same one
- group_gate: float32 [1024], P('ep'), may hold values from 0.2 to 1
- inner_gate: float32 [1024, 2], P('ep'), may hold values from 0.1 to 0.9
- w_gate: bfloat16 [4, 4096, 2048], P('ep', None, 'tp'), may hold values from -0.09375 to 0.09375
- w_up: bfloat16 [4, 4096, 2048], P('ep', None, 'tp'), may hold values from -0.09375 to 0.09375
- w_down: bfloat16 [4, 2048, 4096], P('ep', 'tp'), may hold values from -0.125 to 0.125
Outputs:
- token_grad: bfloat16 [1024, 4096], P('ep', 'tp')
- group_grad: float32 [1024], P('ep')
- inner_grad: float32 [1024, 2], P('ep')
- gate_weight_grad: bfloat16 [4, 4096, 2048], P('ep', None, 'tp')
- up_weight_grad: bfloat16 [4, 4096, 2048], P('ep', None, 'tp')
- down_weight_grad: bfloat16 [4, 2048, 4096], P('ep', 'tp')
Inputs may be any that keep to these rules, and one draw needn't show every extreme that they name: `routing`: each row names 2 different experts. Among the rows of one device (aligned blocks of 256 rows) no expert is named more than 160 times, and in every draw some expert is named exactly 160 times in some block.
All inputs are finite; a program needn't handle non-finite values.
Results may differ from a plain program's by a relative error of at most 0.02.
Values may be sent and summed in bfloat16 or wider, within the bound.
A program may use at most 128 MiB of HBM per device.

v0:
```python
import jax
import jax.numpy as jnp
from jax import lax
from jax.sharding import PartitionSpec as P


def per_device(tokens, cotangent, routing, group_gate, inner_gate, w_gate, w_up, w_down):
    expert_count = lax.axis_size("ep")
    tok_rows, model_width = tokens.shape
    top_k = routing.shape[1]
    capacity = tok_rows * top_k * 5 // (4 * expert_count)
    flat_route = routing.reshape(-1)
    one_hot = (flat_route[:, None] == jnp.arange(expert_count, dtype=jnp.int32)[None, :]).astype(
        jnp.int32
    )
    within = jnp.sum(one_hot * (jnp.cumsum(one_hot, axis=0) - 1), axis=1)
    slot_of = flat_route * capacity + within
    token_of = jnp.arange(tok_rows * top_k, dtype=jnp.int32) // top_k
    combine = (group_gate[:, None] * inner_gate).reshape(-1)
    send_weight = jnp.zeros((expert_count * capacity,), jnp.float32).at[slot_of].set(combine)

    def place_rows(source):
        empty = jnp.zeros((expert_count * capacity, source.shape[1]), source.dtype)
        return empty.at[slot_of].set(source[token_of])

    col_width = model_width // lax.axis_size("tp")
    offset = lax.axis_index("tp") * col_width
    token_cols = place_rows(lax.dynamic_slice_in_dim(tokens, offset, col_width, 1))
    cot_cols = place_rows(lax.dynamic_slice_in_dim(cotangent, offset, col_width, 1))
    token_cols, cot_cols, row_weight = (
        lax.all_to_all(token_cols, "ep", split_axis=0, concat_axis=0, tiled=True),
        lax.all_to_all(cot_cols, "ep", split_axis=0, concat_axis=0, tiled=True),
        lax.all_to_all(
            send_weight.astype(jnp.bfloat16), "ep", split_axis=0, concat_axis=0, tiled=True
        ).astype(send_weight.dtype),
    )
    rows_in, cot_rows = (
        lax.all_gather(token_cols, "tp", axis=1, tiled=True),
        lax.all_gather(cot_cols, "tp", axis=1, tiled=True),
    )
    gate_weight = w_gate[0]
    up_weight = w_up[0]
    down_weight = w_down[0]
    gate_pre = jnp.dot(rows_in, gate_weight, preferred_element_type=jnp.float32)
    up_pre = jnp.dot(rows_in, up_weight, preferred_element_type=jnp.float32)
    sigmoid_gate = jax.nn.sigmoid(gate_pre)
    silu_gate = gate_pre * sigmoid_gate
    hidden = (silu_gate * up_pre).astype(jnp.bfloat16)
    scaled_cot = (row_weight[:, None] * cot_rows).astype(jnp.bfloat16)
    down_grad = lax.dot_general(
        hidden, scaled_cot, (((0,), (0,)), ((), ())), preferred_element_type=jnp.float32
    )
    grad_hidden = lax.dot_general(
        cot_rows, down_weight, (((1,), (1,)), ((), ())), preferred_element_type=jnp.float32
    )
    partial_scores = jnp.sum(grad_hidden * hidden.astype(jnp.float32), axis=1)
    weighted = row_weight[:, None] * grad_hidden
    grad_gate_in = (
        weighted * up_pre * sigmoid_gate * (1.0 + gate_pre * (1.0 - sigmoid_gate))
    ).astype(jnp.bfloat16)
    grad_up_in = (weighted * silu_gate).astype(jnp.bfloat16)
    gate_grad = lax.dot_general(
        rows_in, grad_gate_in, (((0,), (0,)), ((), ())), preferred_element_type=jnp.float32
    )
    upper_grad = lax.dot_general(
        rows_in, grad_up_in, (((0,), (0,)), ((), ())), preferred_element_type=jnp.float32
    )
    partial_rows = lax.dot_general(
        grad_gate_in, gate_weight, (((1,), (1,)), ((), ())), preferred_element_type=jnp.float32
    ) + lax.dot_general(
        grad_up_in, up_weight, (((1,), (1,)), ((), ())), preferred_element_type=jnp.float32
    )
    row_grad = lax.psum_scatter(
        partial_rows.astype(jnp.bfloat16), "tp", scatter_dimension=1, tiled=True
    )
    scores = lax.psum(partial_scores, "tp")
    back_rows, back_scores = (
        lax.all_to_all(row_grad, "ep", split_axis=0, concat_axis=0, tiled=True),
        lax.all_to_all(
            scores.astype(jnp.bfloat16), "ep", split_axis=0, concat_axis=0, tiled=True
        ).astype(scores.dtype),
    )
    picked = back_rows[slot_of].astype(jnp.float32)
    token_grad = jnp.sum(picked.reshape(tok_rows, top_k, picked.shape[1]), axis=1).astype(
        jnp.bfloat16
    )
    score_of = back_scores[slot_of].reshape(tok_rows, top_k)
    inner_grad = group_gate[:, None] * score_of
    group_grad = jnp.sum(inner_gate * score_of, axis=1)
    return (
        token_grad,
        group_grad,
        inner_grad,
        gate_grad.astype(jnp.bfloat16)[None],
        upper_grad.astype(jnp.bfloat16)[None],
        down_grad.astype(jnp.bfloat16)[None],
    )


def solution(mesh):
    return jax.shard_map(
        per_device,
        mesh=mesh,
        in_specs=(
            P("ep", None),
            P("ep", None),
            P("ep", None),
            P("ep"),
            P("ep", None),
            P("ep", None, "tp"),
            P("ep", None, "tp"),
            P("ep", "tp", None),
        ),
        out_specs=(
            P("ep", "tp"),
            P("ep"),
            P("ep", None),
            P("ep", None, "tp"),
            P("ep", None, "tp"),
            P("ep", "tp", None),
        ),
        check_vma=False,
    )
```

profile of v0, /device:TPU:0, one launch (start us, length us, event | category | flops | bytes accessed | tf_op | source)
XLA Modules:
  0.0 238.5 jit_solution(333309969247349896)
XLA Ops:
  7.3 0.8 broadcast_multiply_fusion.2
  8.1 0.8 copy.21
  9.5 1.2 reduce-window.6
  10.7 0.2 slice_reduce_fusion
  11.3 1.1 constant_dynamic-slice_fusion
  12.3 4.9 %scatter_custom_fusion.2 = bf16[640,512]{1,0:T(8,128)(2,1)S(1)} fusion(s32[512]{0:T(512)S(1)} %bitcast.64, bf16[256,512]{1,0:T(8,128)(2,1)S(1)} %get-tuple-element.24, s32[1024]{0:T(1024)S(1)} %pad_clamp_fusion.1, bf16[]{:T(256)} %constant.39.clone.1), kind=kCustom, calls=%fused_computation.32 | custom fusion | bytes 655362 | tf_op jit(solution)/shard_map/scatter | solution.py:24
  17.2 15.0 %all_to_all.56 = bf16[4,160,512]{2,1,0:T(8,128)(2,1)} all-to-all(bf16[4,160,512]{2,1,0:T(8,128)(2,1)S(1)} %bitcast.62), channel_id=1, replica_groups=mesh['ep'=4,'tp'=8] {'ep'}, dimensions={0} | all-to-all | bytes 1310720 | tf_op jit(solution)/shard_map/all_to_all | solution.py:31
  32.3 4.9 %scatter_custom_fusion.1 = bf16[640,512]{1,0:T(8,128)(2,1)S(1)} fusion(s32[512]{0:T(512)S(1)} %bitcast.65, bf16[256,512]{1,0:T(8,128)(2,1)S(1)} %get-tuple-element.25, s32[1024]{0:T(1024)S(1)} %pad_clamp_fusion.1, bf16[]{:T(256)} %constant.39.clone.1), kind=kCustom, calls=%fused_computation.34 | custom fusion | bytes 655362 | tf_op jit(solution)/shard_map/scatter | solution.py:24
  37.2 11.8 %all_to_all.57 = bf16[4,160,512]{2,1,0:T(8,128)(2,1)} all-to-all(bf16[4,160,512]{2,1,0:T(8,128)(2,1)S(1)} %bitcast.61), channel_id=1, replica_groups=mesh['ep'=4,'tp'=8] {'ep'}, dimensions={0} | all-to-all | bytes 1310720 | tf_op jit(solution)/shard_map/all_to_all | solution.py:32
  49.5 2.4 %scatter_custom_fusion = f32[640]{0:T(1024)S(1)} fusion(s32[512]{0:T(512)S(1)} %bitcast.66, f32[512]{0:T(512)S(1)} %reshape.172, f32[]{:T(128)} %constant.17.clone.1), kind=kCustom, calls=%fused_computation.59 | custom fusion | bytes 2564 | tf_op jit(solution)/shard_map/scatter | solution.py:20
  52.1 7.0 %all_to_all.58 = bf16[4,160,1]{1,2,0:T(2,128)(2,1)S(1)} all-to-all(bf16[4,160,1]{1,2,0:T(2,128)(2,1)S(1)} %all_to_all.49), channel_id=1, replica_groups=mesh['ep'=4,'tp'=8] {'ep'}, dimensions={0} | all-to-all | bytes 2560 | tf_op jit(solution)/shard_map/all_to_all | solution.py:33
  59.2 28.9 %all-gather.5.cloned.1.call-done = bf16[640,4096]{1,0:T(8,128)(2,1)} async-done(((bf16[640,512]{1,0:T(8,128)(2,1)}), bf16[640,4096]{1,0:T(8,128)(2,1)}) %all-gather.5.cloned.1.call-update) | async-done | bytes 5242896 | tf_op jit(solution)/shard_map/all_gather | solution.py:38
  88.1 5.3 %fusion.8 = f32[640,256]{0,1:T(8,128)} fusion(bf16[640,4096]{1,0:T(8,128)(2,1)} %all-gather.5.cloned.1.call-done, bf16[1,4096,256]{2,1,0:T(8,128)(2,1)S(1)} %copy-done), kind=kOutput, calls=%fused_computation.19 | convolution fusion | flops 1342177280 | bytes 7995392 | tf_op jit(solution)/shard_map/dot_general | solution.py:44
  93.4 2.8 %fusion.11 = f32[640,256]{0,1:T(8,128)} fusion(bf16[640,4096]{1,0:T(8,128)(2,1)S(1)} %copy-done.5, bf16[1,4096,256]{2,1,0:T(8,128)(2,1)S(1)} %copy-done.1), kind=kOutput, calls=%fused_computation.22 | convolution fusion | flops 1342177280 | bytes 7995392 | tf_op jit(solution)/shard_map/dot_general | solution.py:45
  96.3 48.2 %all-gather.3.cloned.1.call-done = bf16[640,4096]{1,0:T(8,128)(2,1)} async-done(((bf16[640,512]{1,0:T(8,128)(2,1)}), bf16[640,4096]{1,0:T(8,128)(2,1)}) %all-gather.3.cloned.1.call-update) | async-done | bytes 5242896 | tf_op jit(solution)/shard_map/all_gather | solution.py:39
  144.5 5.4 %multiply_reduce_fusion = (f32[640]{0:T(1024)S(1)}, bf16[640,256]{0,1:T(8,128)(2,1)S(1)}, bf16[640,256]{0,1:T(8,128)(2,1)S(1)}, bf16[640,256]{0,1:T(8,128)(2,1)S(1)}) fusion(f32[640,256]{0,1:T(8,128)} %fusion.11, f32[640,256]{0,1:T(8,128)} %fusion.8, f32[640]{0:T(1024)S(1)} %reshape.134, bf16[640,4096]{1,0:T(8,128)(2,1)} %all-gather.3.cloned.1.call-done, ...), kind=kOutput, calls=%fused_computation.26 | convolution fusion | flops 1345289600 | bytes 9638912 | tf_op jit(solution)/shard_map/dot_general | solution.py:53
  149.9 1.6 fusion.6
  151.5 4.1 %add_convert_fusion = bf16[640,4096]{1,0:T(8,128)(2,1)} fusion(f32[640,4096]{1,0:T(8,128)S(1)} %fusion.6, bf16[640,256]{0,1:T(8,128)(2,1)S(1)} %get-tuple-element.21, bf16[1,4096,256]{2,1,0:T(8,128)(2,1)S(1)} %copy-done.2), kind=kOutput, calls=%fused_computation.8 | convolution fusion | flops 1347420160 | bytes 18153472 | tf_op jit(solution)/shard_map/dot_general | solution.py:70
  155.7 14.8 %psum.7 = bf16[640]{0:T(1024)(128)(2,1)S(1)} all-reduce(f32[640]{0:T(1024)S(1)} %get-tuple-element.18), channel_id=1, replica_groups=mesh['ep'=4,'tp'=8] {'tp'}, use_global_device_ids=true, to_apply=%region_9.10 | all-reduce | flops 640 | bytes 3840 | tf_op jit(solution)/shard_map/psum | solution.py:76
  170.5 0.7 all_to_all.50
  171.2 3.9 %all-to-all-start.4 = ((bf16[4,160,1]{1,2,0:T(2,128)(2,1)}), bf16[4,160,1]{1,2,0:T(2,128)(2,1)S(1)}, u32[]{:S(2)}, u32[]{:S(2)}) async-start(bf16[4,160,1]{1,2,0:T(2,128)(2,1)} %all_to_all.50), calls=%async_computation.5 | async-start | bytes 8192 | tf_op jit(solution)/shard_map/all_to_all | solution.py:79
  175.0 5.7 %fusion.5 = bf16[1,256,4096]{2,1,0:T(8,128)(2,1)} fusion(bf16[640,256]{0,1:T(8,128)(2,1)S(1)} %get-tuple-element.19, bf16[640,4096]{1,0:T(8,128)(2,1)} %all-gather.3.cloned.1.call-done, f32[640]{0:T(1024)S(1)} %reshape.134), kind=kOutput, calls=%fused_computation.16 | convolution fusion | flops 1351090176 | bytes 7670272 | tf_op jit(solution)/shard_map/dot_general | solution.py:50
  180.8 5.7 %fusion.3 = bf16[1,4096,256]{2,1,0:T(8,128)(2,1)} fusion(bf16[640,4096]{1,0:T(8,128)(2,1)} %all-gather.5.cloned.1.call-done, bf16[640,256]{0,1:T(8,128)(2,1)S(1)} %get-tuple-element.20), kind=kOutput, calls=%fused_computation.14 | convolution fusion | flops 1343225856 | bytes 7667712 | tf_op jit(solution)/shard_map/dot_general | solution.py:62
  186.5 28.0 %reduce-scatter.2.cloned.1.call-done = bf16[640,512]{1,0:T(8,128)(2,1)} async-done(((bf16[640,4096]{1,0:T(8,128)(2,1)}), bf16[640,512]{1,0:T(8,128)(2,1)}) %reduce-scatter.2.cloned.1.call-update) | async-done | bytes 655376 | tf_op jit(solution)/shard_map/reduce_scatter | solution.py:73
  214.5 3.6 %all-to-all-start.3 = ((bf16[4,160,512]{2,1,0:T(8,128)(2,1)}), bf16[4,160,512]{2,1,0:T(8,128)(2,1)S(1)}, u32[]{:S(2)}, u32[]{:S(2)}) async-start(bf16[4,160,512]{2,1,0:T(8,128)(2,1)} %bitcast.63), calls=%async_computation.4 | async-start | bytes 1310720 | tf_op jit(solution)/shard_map/all_to_all | solution.py:78
  218.2 5.7 %fusion.4 = bf16[1,4096,256]{2,1,0:T(8,128)(2,1)} fusion(bf16[640,4096]{1,0:T(8,128)(2,1)} %all-gather.5.cloned.1.call-done, bf16[640,256]{0,1:T(8,128)(2,1)S(1)} %get-tuple-element.21), kind=kOutput, calls=%fused_computation.15 | convolution fusion | flops 1343225856 | bytes 7667712 | tf_op jit(solution)/shard_map/dot_general | solution.py:65
  223.9 2.3 gather_fusion.1
  226.4 0.7 broadcast_multiply_fusion
  227.0 0.7 copy.27
  227.7 2.0 gather_fusion
  229.7 0.2 gather.17
  229.9 2.1 reduce_sum.43
  (42 shorter events, 1.9 us)
Async XLA Ops:
  7.2 81.0 %copy-start = (bf16[1,4096,256]{2,1,0:T(8,128)(2,1)S(1)}, bf16[1,4096,256]{2,1,0:T(8,128)(2,1)}, u32[]{:S(2)}) copy-start(bf16[1,4096,256]{2,1,0:T(8,128)(2,1)} %param.13) | copy-start | bytes 6291460
  7.2 41.9 %copy-start.4 = (f32[256,2]{0,1:T(2,128)S(1)}, f32[256,2]{0,1:T(2,128)}, u32[]{:S(2)}) copy-start(f32[256,2]{0,1:T(2,128)} %param.12) | copy-start | bytes 6148
  7.2 42.1 %copy-start.3 = (f32[256]{0:T(256)S(1)}, f32[256]{0:T(256)}, u32[]{:S(2)}) copy-start(f32[256]{0:T(256)} %param.11) | copy-start | bytes 3076
  7.2 80.9 %all-gather.5.cloned.1.call-start = ((), (), s32[]{:S(2)}) async-start(), calls=%async_computation.7 | async-start | bytes 5898240 | tf_op jit(solution)/shard_map/all_gather | solution.py:38
  32.3 112.2 %all-gather.3.cloned.1.call-start = ((), (), s32[]{:S(2)}) async-start(), calls=%async_computation.6 | async-start | bytes 5898240 | tf_op jit(solution)/shard_map/all_gather | solution.py:39
  49.1 165.4 %reduce-scatter.2.cloned.1.call-start = ((), (), s32[]{:S(2)}) async-start(), calls=%async_computation.8 | async-start | bytes 5898240 | tf_op jit(solution)/shard_map/reduce_scatter | solution.py:73
  88.1 5.3 %copy-start.1 = (bf16[1,4096,256]{2,1,0:T(8,128)(2,1)S(1)}, bf16[1,4096,256]{2,1,0:T(8,128)(2,1)}, u32[]{:S(2)}) copy-start(bf16[1,4096,256]{2,1,0:T(8,128)(2,1)} %param.14) | copy-start | bytes 6291460
  88.1 5.3 %copy-start.5 = (bf16[640,4096]{1,0:T(8,128)(2,1)S(1)}, bf16[640,4096]{1,0:T(8,128)(2,1)}, u32[]{:S(2)}) copy-start(bf16[640,4096]{1,0:T(8,128)(2,1)} %all-gather.5.cloned.1.call-done) | copy-start | bytes 15728644
  149.9 1.6 copy-start.2
  171.2 15.3 %all-to-all-start.4 = ((bf16[4,160,1]{1,2,0:T(2,128)(2,1)}), bf16[4,160,1]{1,2,0:T(2,128)(2,1)S(1)}, u32[]{:S(2)}, u32[]{:S(2)}) async-start(bf16[4,160,1]{1,2,0:T(2,128)(2,1)} %all_to_all.50), calls=%async_computation.5 | async-start | bytes 8192 | tf_op jit(solution)/shard_map/all_to_all | solution.py:79
  214.5 13.2 %all-to-all-start.3 = ((bf16[4,160,512]{2,1,0:T(8,128)(2,1)}), bf16[4,160,512]{2,1,0:T(8,128)(2,1)S(1)}, u32[]{:S(2)}, u32[]{:S(2)}) async-start(bf16[4,160,512]{2,1,0:T(8,128)(2,1)} %bitcast.63), calls=%async_computation.4 | async-start | bytes 1310720 | tf_op jit(solution)/shard_map/all_to_all | solution.py:78
Sparse Core Ops, SparseCore 0:
  32.4 55.6 all-gather.4
  89.7 54.7 all-gather.2
  155.8 58.7 reduce-scatter.1
where the time goes:
time: 239 us; the launch traced here: 238 us
  waiting for transfers between devices  105 us (44%)
  blocking collectives  48.7 us (20%)
  matrix products  36.3 us (15%)
  local copies, waits for them, and re-layouts  21.4 us (9%)
  between operations  14 us (6%)
  starting transfers between devices  7.63 us (3%)
  other arithmetic  5.27 us (2%)
    all_gather x1, waiting for transfers between devices, per_device(): lax.all_gather(cot_cols, 'tp', axis=1, tiled=True)  48.2 us
    all_gather x1, waiting for transfers between devices, per_device(): lax.all_gather(token_cols, 'tp', axis=1, tiled=True)  28.9 us
    reduce_scatter x1, waiting for transfers between devices, per_device(): lax.psum_scatter(partial_rows.astype(jnp.bfloat16), 'tp', scatter_dimensi...  28 us
    all_to_all x1, blocking collectives, per_device(): lax.all_to_all(token_cols, 'ep', split_axis=0, concat_axis=0, tiled=True)  15 us
    psum x1, blocking collectives, per_device(): scores = lax.psum(partial_scores, 'tp')  14.8 us
    all_to_all x1, blocking collectives, per_device(): lax.all_to_all(cot_cols, 'ep', split_axis=0, concat_axis=0, tiled=True)  11.8 us
    scatter x2, local copies, waits for them, and re-layouts, place_rows(): return empty.at[slot_of].set(source[token_of])  9.78 us
    all_to_all x1, blocking collectives, per_device(): lax.all_to_all(send_weight.astype(jnp.bfloat16), 'ep', split_axis=0, conc...  7.01 us
  transfers between devices with their start and end apart: 5, of which 3 were waited for; matrix products, arithmetic and copies ran while one was open for 15% of the time, Pallas kernels for 0%

commit v1 on v0

v1 whole, which is shorter than its diff:
```python
import functools

import jax
import jax.numpy as jnp
from jax import lax
from jax.experimental import pallas as pl
from jax.experimental.pallas import tpu as pltpu
from jax.sharding import PartitionSpec as P

LANES = 128
BF16 = jnp.bfloat16
F32 = jnp.float32


def peer_of(me, d, n):
    if n & (n - 1):
        return lax.rem(2 * n + d - me, n)
    out, bit = me, 1
    while bit < n:
        if d & bit:
            out = out + bit * (1 - 2 * lax.rem(me // bit, 2))
        bit *= 2
    return out


def barrier(partners):
    sem = pltpu.get_barrier_semaphore()
    for ep, tp in partners:
        pl.semaphore_signal(
            sem, inc=1, device_id=(ep, tp), device_id_type=pl.DeviceIdType.MESH
        )
    pl.semaphore_wait(sem, len(partners))


def remote(src, dst, send, recv, ep, tp):
    return pltpu.make_async_remote_copy(
        src_ref=src,
        dst_ref=dst,
        send_sem=send,
        recv_sem=recv,
        device_id=(ep, tp),
        device_id_type=pl.DeviceIdType.MESH,
    )


def dispatch_kernel(n_ep, n_tp, xs, gs, cs, x_out, g_out, c_out, send, recv, c_send, c_recv, stage, local):
    ep, tp = lax.axis_index("ep"), lax.axis_index("tp")
    core = lax.rem(tp, 2)
    z = tp // 2
    sibling = tp + 1 - 2 * core
    odd = lax.rem(z, 2)
    across = tp + 2 - 4 * odd
    half = xs.shape[2] // 2
    blocks = half // LANES
    lone = blocks * 3 // 8 * LANES
    both = half - 2 * lone
    base = core * half
    peers = [peer_of(ep, d, n_ep) for d in range(1, n_ep)]
    barrier([(p, tp) for p in peers] + [(ep, sibling), (ep, across)])

    def cols(start, width):
        return pl.ds(pl.multiple_of(start, LANES), width)

    mine = cols(base + odd * (lone + both), lone)
    theirs = cols(base + (1 - odd) * (lone + both), lone)
    shared = cols(base + lone, both)

    pairs = ((xs, x_out), (gs, g_out))
    started, direct = [], {}
    for d, p in enumerate(peers):
        copy = remote(cs.at[p], c_out.at[ep], c_send.at[d], c_recv.at[d], p, tp)
        copy.start()
        started.append(copy)
    for a, (src, dst) in enumerate(pairs):
        for kind, part in ((0, mine), (1, shared)):
            for d, p in enumerate(peers):
                copy = remote(
                    src.at[p, :, part], dst.at[ep, :, part],
                    send.at[a, d, kind], recv.at[a, d, kind], p, tp,
                )
                copy.start()
                direct[a, kind, d] = copy
    loads = []
    for a, (src, dst) in enumerate(pairs):
        load = pltpu.make_async_copy(src.at[ep], stage.at[a], local.at[a])
        load.start()
        loads.append(load)
    load = pltpu.make_async_copy(cs.at[ep], stage_c(c_out, ep), local.at[4])
    load.start()
    stores = [load]
    for a, (src, dst) in enumerate(pairs):
        loads[a].wait()
        store = pltpu.make_async_copy(stage.at[a], dst.at[ep], local.at[2 + a])
        store.start()
        stores.append(store)

    forwards = []
    for a, (src, dst) in enumerate(pairs):
        for kind, part in ((0, mine), (1, shared)):
            for d, p in enumerate(peers):
                direct[a, kind, d].wait_recv()
                if kind == 0:
                    copy = remote(
                        dst.at[p, :, part], dst.at[p, :, part],
                        send.at[a, d, 2], recv.at[a, d, 2], ep, across,
                    )
                    copy.start()
                    forwards.append(copy)
                    direct[a, 2, d] = remote(
                        dst.at[p, :, theirs], dst.at[p, :, theirs],
                        send.at[a, d, 2], recv.at[a, d, 2], ep, across,
                    )
                copy = remote(
                    dst.at[p, :, part], dst.at[p, :, part],
                    send.at[a, d, 3 + kind], recv.at[a, d, 3 + kind], ep, sibling,
                )
                copy.start()
                forwards.append(copy)
    for a, (src, dst) in enumerate(pairs):
        for d, p in enumerate(peers):
            direct[a, 2, d].wait_recv()
            copy = remote(
                dst.at[p, :, theirs], dst.at[p, :, theirs],
                send.at[a, d, 5], recv.at[a, d, 5], ep, sibling,
            )
            copy.start()
            forwards.append(copy)
    for a, (src, dst) in enumerate(pairs):
        for d, p in enumerate(peers):
            for kind, offset, width in (
                (3, odd * (lone + both), lone),
                (4, lone, both),
                (5, (1 - odd) * (lone + both), lone),
            ):
                part = cols((1 - core) * half + offset, width)
                remote(
                    dst.at[p, :, part], dst.at[p, :, part],
                    send.at[a, d, kind], recv.at[a, d, kind], ep, sibling,
                ).wait_recv()
    for copy in started:
        copy.wait()
    for key, copy in direct.items():
        if key[1] != 2:
            copy.wait_send()
    for copy in forwards:
        copy.wait_send()
    for store in stores:
        store.wait()


def stage_c(c_out, ep):
    return c_out.at[ep]


def dispatch(n_ep, n_tp, xs, gs, cs):
    any_spec = pl.BlockSpec(memory_space=pl.ANY)
    return pl.pallas_call(
        functools.partial(dispatch_kernel, n_ep, n_tp),
        out_shape=(
            jax.ShapeDtypeStruct(xs.shape, xs.dtype),
            jax.ShapeDtypeStruct(gs.shape, gs.dtype),
            jax.ShapeDtypeStruct(cs.shape, cs.dtype),
        ),
        in_specs=[any_spec] * 3,
        out_specs=(any_spec,) * 3,
        scratch_shapes=[
            pltpu.SemaphoreType.DMA((2, n_ep - 1, 6)),
            pltpu.SemaphoreType.DMA((2, n_ep - 1, 6)),
            pltpu.SemaphoreType.DMA((n_ep - 1,)),
            pltpu.SemaphoreType.DMA((n_ep - 1,)),
            pltpu.VMEM((2,) + xs.shape[1:], xs.dtype),
            pltpu.SemaphoreType.DMA((5,)),
        ],
        compiler_params=pltpu.CompilerParams(collective_id=0, has_side_effects=True),
    )(xs, gs, cs)


def return_kernel(n_ep, n_tp, gg, gu, wg, wu, pick, sc, out, sc_out,
                  first, first_in, second, second_in, third, third_in,
                  s1, r1, s2, r2, s3, r3, ss, rs, sl):
    ep, tp = lax.axis_index("ep"), lax.axis_index("tp")
    core = lax.rem(tp, 2)
    z = tp // 2
    nz = n_tp // 2
    sibling = tp + 1 - 2 * core
    width = out.shape[1]
    cap = second.shape[2]
    peers = [peer_of(ep, d, n_ep) for d in range(1, n_ep)]
    everyone = [(p, tp) for p in peers]
    everyone += [(ep, lax.rem(tp + k, n_tp)) for k in range(1, n_tp)]
    score_to = [(p, lax.rem(tp + k, n_tp)) for p in [ep] + peers for k in range(n_tp)][1:]
    barrier(score_to)

    sends = []
    for i, (p, t) in enumerate(score_to):
        copy = remote(sc.at[p], sc_out.at[ep, tp], ss.at[i], rs.at[i], p, t)
        copy.start()
        sends.append(copy)
    own_score = pltpu.make_async_copy(sc.at[ep], sc_out.at[ep, tp], sl)
    own_score.start()

    def partial(share):
        rows = pl.ds(pl.multiple_of(share * width, width), width)
        dims = (((1,), (1,)), ((), ()))
        return lax.dot_general(
            gg[...], wg[rows, :], dims, preferred_element_type=F32
        ) + lax.dot_general(gu[...], wu[rows, :], dims, preferred_element_type=F32)

    order = [lax.rem(z + dz, nz) for dz in range(nz - 1, -1, -1)]
    halves = []
    for i, zz in enumerate(order):
        first[i] = partial(2 * zz + 1 - core).astype(BF16)
        copy = remote(first.at[i], first_in.at[i], s1.at[i], r1.at[i], ep, sibling)
        copy.start()
        halves.append(copy)
    moves = {}
    for i, zz in enumerate(order):
        total = partial(2 * zz + core)
        halves[i].wait_recv()
        total = total + first_in[i].astype(F32)
        second[i] = total.astype(BF16).reshape(second.shape[1:])
        for d, p in enumerate(peers):
            copy = remote(
                second.at[i, p], second_in.at[i, ep], s2.at[i, d], r2.at[i, d], p, tp
            )
            copy.start()
            moves[i, d] = copy
    last = []
    for i, zz in enumerate(order):
        for d, p in enumerate(peers):
            moves[i, d].wait_recv()
        second_in[i, ep] = second[i, ep]
        rows = second_in[i].reshape(n_ep * cap, width)
        summed = jnp.dot(pick[...], rows, preferred_element_type=F32)
        third[i] = summed.astype(BF16)
        if i < nz - 1:
            copy = remote(
                third.at[i], third_in.at[i], s3.at[i], r3.at[i], ep, 2 * zz + core
            )
            copy.start()
            last.append(copy)
    total = third[nz - 1].astype(F32)
    for i in range(nz - 1):
        last[i].wait_recv()
        total = total + third_in[i].astype(F32)
    out[...] = total.astype(BF16)
    for copy in halves + list(moves.values()) + last:
        copy.wait_send()
    for copy in sends:
        copy.wait()
    own_score.wait()


def give_back(n_ep, n_tp, gg, gu, wg, wu, pick, sc):
    vmem = pl.BlockSpec(memory_space=pltpu.VMEM)
    any_spec = pl.BlockSpec(memory_space=pl.ANY)
    rows, nz = gg.shape[0], n_tp // 2
    width = wg.shape[0] // n_tp
    tokens = pick.shape[0]
    cap = rows // n_ep
    dma = pltpu.SemaphoreType.DMA
    others = n_ep * n_tp - 1
    return pl.pallas_call(
        functools.partial(return_kernel, n_ep, n_tp),
        out_shape=(
            jax.ShapeDtypeStruct((tokens, width), BF16),
            jax.ShapeDtypeStruct((n_ep, n_tp) + sc.shape[1:], F32),
        ),
        in_specs=[vmem] * 5 + [any_spec],
        out_specs=(vmem, any_spec),
        scratch_shapes=[
            pltpu.VMEM((nz, rows, width), BF16),
            pltpu.VMEM((nz, rows, width), BF16),
            pltpu.VMEM((nz, n_ep, cap, width), BF16),
            pltpu.VMEM((nz, n_ep, cap, width), BF16),
            pltpu.VMEM((nz, tokens, width), BF16),
            pltpu.VMEM((nz, tokens, width), BF16),
            dma((nz,)), dma((nz,)),
            dma((nz, n_ep - 1)), dma((nz, n_ep - 1)),
            dma((nz,)), dma((nz,)),
            dma((others,)), dma((others,)),
            dma,
        ],
        compiler_params=pltpu.CompilerParams(
            collective_id=1, has_side_effects=True, vmem_limit_bytes=56 * 1024 * 1024
        ),
    )(gg, gu, wg, wu, pick, sc)


def per_device(tokens, cotangent, routing, group_gate, inner_gate, w_gate, w_up, w_down):
    n_ep, n_tp = lax.axis_size("ep"), lax.axis_size("tp")
    tok_rows, model_width = tokens.shape
    top_k = routing.shape[1]
    cap = tok_rows * top_k * 5 // (4 * n_ep)
    rows = n_ep * cap
    experts = jnp.arange(n_ep, dtype=jnp.int32)
    route_t = routing.T
    names = jnp.sum((route_t[:, None, :] == experts[None, :, None]).astype(F32), axis=0)
    place = jnp.arange(tok_rows)
    before = (place[:, None] < place[None, :]).astype(BF16)
    rank = jnp.dot(names.astype(BF16), before, preferred_element_type=F32).astype(jnp.int32)
    slot_t = jnp.sum(
        jnp.where(
            route_t[:, None, :] == experts[None, :, None],
            experts[None, :, None] * cap + rank[None],
            0,
        ),
        axis=1,
    )
    slots = jnp.arange(rows, dtype=jnp.int32)
    hits = slots[:, None, None] == slot_t[None]
    put = jnp.any(hits, axis=1).astype(BF16)
    combine = (group_gate[:, None] * inner_gate).T
    weight = jnp.sum(jnp.where(hits, combine[None], 0.0), axis=(1, 2))
    pad = -cap % LANES
    send_weight = jnp.pad(weight.reshape(n_ep, 1, cap), ((0, 0), (0, 0), (0, pad)))

    def placed(source):
        return jnp.dot(put, source, preferred_element_type=F32).astype(BF16).reshape(
            n_ep, cap, model_width
        )

    rows_in, cot_rows, weight_in = dispatch(
        n_ep, n_tp, placed(tokens), placed(cotangent), send_weight
    )
    rows_in = rows_in.reshape(rows, model_width)
    cot_rows = cot_rows.reshape(rows, model_width)
    row_weight = weight_in[:, 0, :cap].reshape(rows)

    gate_weight, up_weight, down_weight = w_gate[0], w_up[0], w_down[0]
    gate_pre = jnp.dot(rows_in, gate_weight, preferred_element_type=F32)
    up_pre = jnp.dot(rows_in, up_weight, preferred_element_type=F32)
    sigmoid_gate = jax.nn.sigmoid(gate_pre)
    silu_gate = gate_pre * sigmoid_gate
    hidden = (silu_gate * up_pre).astype(BF16)
    scaled_cot = (row_weight[:, None] * cot_rows).astype(BF16)
    down_grad = lax.dot_general(
        hidden, scaled_cot, (((0,), (0,)), ((), ())), preferred_element_type=F32
    )
    grad_hidden = lax.dot_general(
        cot_rows, down_weight, (((1,), (1,)), ((), ())), preferred_element_type=F32
    )
    partial_scores = jnp.sum(grad_hidden * hidden.astype(F32), axis=1)
    weighted = row_weight[:, None] * grad_hidden
    grad_gate_in = (
        weighted * up_pre * sigmoid_gate * (1.0 + gate_pre * (1.0 - sigmoid_gate))
    ).astype(BF16)
    grad_up_in = (weighted * silu_gate).astype(BF16)
    gate_grad = lax.dot_general(
        rows_in, grad_gate_in, (((0,), (0,)), ((), ())), preferred_element_type=F32
    )
    upper_grad = lax.dot_general(
        rows_in, grad_up_in, (((0,), (0,)), ((), ())), preferred_element_type=F32
    )
    send_score = jnp.pad(
        partial_scores.reshape(n_ep, 1, cap), ((0, 0), (0, 0), (0, pad))
    )
    token_grad, all_scores = give_back(
        n_ep, n_tp, grad_gate_in, grad_up_in, gate_weight, up_weight, put.T, send_score
    )
    scores = jnp.sum(all_scores[:, :, 0, :cap], axis=1).reshape(rows)
    score_t = jnp.sum(jnp.where(hits, scores[:, None, None], 0.0), axis=0)
    score_of = score_t.T
    inner_grad = group_gate[:, None] * score_of
    group_grad = jnp.sum(inner_gate * score_of, axis=1)
    return (
        token_grad,
        group_grad,
        inner_grad,
        gate_grad.astype(BF16)[None],
        upper_grad.astype(BF16)[None],
        down_grad.astype(BF16)[None],
    )


def solution(mesh):
    return jax.shard_map(
        per_device,
        mesh=mesh,
        in_specs=(
            P("ep", None),
            P("ep", None),
            P("ep", None),
            P("ep"),
            P("ep", None),
            P("ep", None, "tp"),
            P("ep", None, "tp"),
            P("ep", "tp", None),
        ),
        out_specs=(
            P("ep", "tp"),
            P("ep"),
            P("ep", None),
            P("ep", None, "tp"),
            P("ep", None, "tp"),
            P("ep", "tp", None),
        ),
        check_vma=False,
    )
```

time: 239 us -> 139 us (0.58)
  waiting for transfers between devices: 105 us -> 0 us
  Pallas kernels: 0 us -> 93.5 us
  blocking collectives: 48.7 us -> 0 us
  local copies, waits for them, and re-layouts: 21.4 us -> 3.99 us
  between operations: 14 us -> 0.78 us
  starting transfers between devices: 7.63 us -> 0 us
    pallas_call x0 -> x2, Pallas kernels: none -> 93.5 us  [the longest x1 47.9 us: dispatch(): pl.pallas_call(functools.partial(dispatch_kernel, n_ep, n_tp), out_shape=...]
    all_gather x2 -> x0, waiting for transfers between devices: 77.2 us -> none  [the longest x1 48.2 us: per_device(): lax.all_gather(cot_cols, 'tp', axis=1, tiled=True)]
    all_to_all x3 -> x0, blocking collectives: 33.9 us -> none  [the longest x1 15 us: per_device(): lax.all_to_all(token_cols, 'ep', split_axis=0, concat_axis=0, tiled=True)]
    reduce_scatter x1 -> x0, waiting for transfers between devices: 28 us -> none  [per_device(): lax.psum_scatter(partial_rows.astype(jnp.bfloat16), 'tp', scatter_dimensi...]
    psum x1 -> x0, blocking collectives: 14.8 us -> none  [per_device(): scores = lax.psum(partial_scores, 'tp')]
    scatter x3 -> x0, local copies, waits for them, and re-layouts: 12.2 us -> none  [the longest x2 9.78 us: place_rows(): return empty.at[slot_of].set(source[token_of])]
    all_to_all x2 -> x0, starting transfers between devices: 7.51 us -> none  [the longest x1 3.87 us: per_device(): lax.all_to_all(scores.astype(jnp.bfloat16), 'ep', split_axis=0, concat_ax...]
    gather x3 -> x0, local copies, waits for them, and re-layouts: 4.44 us -> none  [the longest x1 2.28 us: per_device(): score_of = back_scores[slot_of].reshape(tok_rows, top_k)]
  transfers between devices with their start and end apart: 5 -> 0, of which waited for: 3 -> 0; matrix products, arithmetic and copies ran while one was open for 15% -> 0% of each run, Pallas kernels for 0% -> 0%
where the time goes in v1:
time: 139 us
  Pallas kernels  93.5 us (67%)
  matrix products  35.3 us (25%)
  other arithmetic  4.96 us (4%)
  local copies, waits for them, and re-layouts  3.99 us (3%)
    pallas_call x1, Pallas kernels, dispatch(): pl.pallas_call(functools.partial(dispatch_kernel, n_ep, n_tp), out_shape=...  47.9 us
    pallas_call x1, Pallas kernels, give_back(): pl.pallas_call(functools.partial(return_kernel, n_ep, n_tp), out_shape=(j...  45.6 us
    dot_general x2, matrix products, placed(): jnp.dot(put, source, preferred_element_type=F32).astype(BF16)  7.67 us
    dot_general x1, matrix products, per_device(): lax.dot_general(hidden, scaled_cot, (((0,), (0,)), ((), ())), preferred_e...  6.03 us
    dot_general x1, matrix products, per_device(): lax.dot_general(rows_in, grad_up_in, (((0,), (0,)), ((), ())), preferred_...  5.96 us
    dot_general x1, matrix products, per_device(): lax.dot_general(cot_rows, down_weight, (((1,), (1,)), ((), ())), preferre...  5.06 us
    dot_general x1, matrix products, per_device(): gate_pre = jnp.dot(rows_in, gate_weight, preferred_element_type=F32)  4.81 us
    dot_general x1, matrix products, per_device(): lax.dot_general(rows_in, grad_gate_in, (((0,), (0,)), ((), ())), preferre...  3.24 us

profile of v1, /device:TPU:0, one launch (start us, length us, event | category | flops | bytes accessed | tf_op | source)
XLA Modules:
  0.0 138.5 jit_solution(4988293632361088342)
XLA Ops:
  0.6 0.0 copy-start
  0.6 0.8 convert_reduce_fusion
  1.5 0.1 fusion.9
  1.6 0.7 select_reduce_fusion.2
  2.4 0.2 fusion.8
  2.6 0.0 copy-start.2
  2.6 3.9 %convolution_convert_fusion.1 = bf16[640,4096]{1,0:T(8,128)(2,1)} fusion(pred[640,256]{1,0:T(8,128)(4,1)S(1)} %fusion.8, bf16[256,4096]{1,0:T(8,128)(2,1)S(1)} %copy-done), kind=kOutput, calls=%fused_computation.2 | convolution fusion | flops 1344798720 | bytes 7503872 | tf_op jit(solution)/shard_map/dot_general | solution.py:319
  6.5 3.8 %convolution_convert_fusion = bf16[640,4096]{1,0:T(8,128)(2,1)} fusion(pred[640,256]{1,0:T(8,128)(4,1)S(1)} %fusion.8, bf16[256,4096]{1,0:T(8,128)(2,1)S(1)} %copy-done.2), kind=kOutput, calls=%fused_computation.1 | convolution fusion | flops 1344798720 | bytes 7503872 | tf_op jit(solution)/shard_map/dot_general | solution.py:319
  10.3 0.2 select_reduce_fusion.1
  10.5 0.1 reshape.47
  10.6 0.6 pad.7.cs
  11.2 47.9 %shard_map.127 = (bf16[4,160,4096]{2,1,0:T(8,128)(2,1)}, bf16[4,160,4096]{2,1,0:T(8,128)(2,1)}, f32[4,1,256]{2,1,0:T(1,128)}) custom-call(bf16[4,160,4096]{2,1,0:T(8,128)(2,1)} %bitcast.44, bf16[4,160,4096]{2,1,0:T(8,128)(2,1)} %bitcast.45, f32[4,1,256]{2,1,0:T(1,128)} %pad.7.cs), custom_call_target="tpu_custom_call" | custom-call | tf_op jit(solution)/shard_map/pallas_call | solution.py:157
  59.1 0.0 copy-start.1
  59.1 4.8 %fusion.13 = f32[640,256]{1,0:T(8,128)S(1)} fusion(bf16[640,4096]{1,0:T(8,128)(2,1)} %bitcast.50, bf16[1,4096,256]{2,1,0:T(8,128)(2,1)} %param.13), kind=kOutput, calls=%fused_computation.38 | convolution fusion | flops 1342177280 | bytes 7995392 | tf_op jit(solution)/shard_map/dot_general | solution.py:331
  64.0 0.4 copy-done.8
  64.4 2.4 %fusion.15 = f32[640,256]{1,0:T(8,128)} fusion(bf16[640,4096]{1,0:T(8,128)(2,1)S(1)} %bitcast.52, bf16[1,4096,256]{2,1,0:T(8,128)(2,1)S(1)} %copy-done.1), kind=kOutput, calls=%fused_computation.40 | convolution fusion | flops 1342177280 | bytes 7995392 | tf_op jit(solution)/shard_map/dot_general | solution.py:332
  66.8 0.1 mul.70
  66.8 5.1 %multiply_reduce_fusion = (f32[640]{0:T(1024)S(1)}, bf16[640,256]{1,0:T(8,128)(2,1)S(1)}, bf16[640,256]{1,0:T(8,128)(2,1)S(1)}, bf16[640,256]{1,0:T(8,128)(2,1)S(1)}) fusion(f32[640,256]{1,0:T(8,128)} %fusion.15, f32[640,256]{1,0:T(8,128)S(1)} %fusion.13, f32[640]{0:T(1024)S(1)} %mul.70, bf16[640,4096]{1,0:T(8,128)(2,1)} %bitcast.56, ...), kind=kOutput, calls=%fused_computation.19 | convolution fusion | flops 1345289600 | bytes 9638912 | tf_op jit(solution)/shard_map/dot_general | solution.py:340
  71.9 0.0 slice-start
  71.9 6.0 %fusion.5 = bf16[1,256,4096]{2,1,0:T(8,128)(2,1)} fusion(bf16[640,256]{1,0:T(8,128)(2,1)S(1)} %get-tuple-element.17, bf16[640,4096]{1,0:T(8,128)(2,1)} %bitcast.57, f32[640]{0:T(1024)S(1)} %mul.70), kind=kOutput, calls=%fused_computation.10 | convolution fusion | flops 1351090176 | bytes 7670272 | tf_op jit(solution)/shard_map/dot_general | solution.py:337
  78.0 6.0 %fusion.4 = bf16[1,4096,256]{2,1,0:T(8,128)(2,1)} fusion(bf16[640,4096]{1,0:T(8,128)(2,1)} %bitcast.51, bf16[640,256]{1,0:T(8,128)(2,1)S(1)} %get-tuple-element.19.gu), kind=kOutput, calls=%fused_computation.9 | convolution fusion | flops 1343225856 | bytes 7667712 | tf_op jit(solution)/shard_map/dot_general | solution.py:352
  84.0 3.2 %fusion.3 = bf16[1,4096,256]{2,1,0:T(8,128)(2,1)} fusion(bf16[640,4096]{1,0:T(8,128)(2,1)S(1)} %bitcast.55, bf16[640,256]{1,0:T(8,128)(2,1)S(1)} %get-tuple-element.18.gg), kind=kOutput, calls=%fused_computation.8 | convolution fusion | flops 1343225856 | bytes 7667712 | tf_op jit(solution)/shard_map/dot_general | solution.py:349
  87.2 0.1 reshape.50
  87.3 0.6 pad.8.sc
  87.9 0.3 copy.26
  88.2 0.7 convert_bitcast_fusion.pick
  88.9 45.6 %shard_map.128 = (bf16[256,512]{1,0:T(8,128)(2,1)}, f32[4,8,1,256]{3,2,1,0:T(1,128)}) custom-call(bf16[640,256]{1,0:T(8,128)(2,1)} %copy-done.3, bf16[640,256]{1,0:T(8,128)(2,1)} %copy-done.4, bf16[4096,256]{1,0:T(8,128)(2,1)} %bitcast.47, bf16[4096,256]{1,0:T(8,128)(2,1)} %bitcast.46, bf16[256,640]{1,0:T(8,128)(2,1)} %convert_bitcast_fusion.pick, ...), custom_call_target="tpu_custom_call" | custom-call | tf_op jit(solution)/shard_map/pallas_call | solution.py:263
  134.6 0.8 slice_reduce_fusion
  135.4 0.1 broadcast_in_dim.62
  135.4 0.3 select_reduce_fusion
  135.7 1.1 bitcast_multiply_fusion
  136.9 1.7 %copy.33 = bf16[256,512]{1,0:T(8,128)(2,1)} copy(bf16[256,512]{1,0:T(8,128)(2,1)} %get-tuple-element.28) | data formatting | bytes 524288
  (21 shorter events, 0.1 us)
Async XLA Ops:
  0.6 2.0 %copy-start = (bf16[256,4096]{1,0:T(8,128)(2,1)S(1)}, bf16[256,4096]{1,0:T(8,128)(2,1)}, u32[]{:S(2)}) copy-start(bf16[256,4096]{1,0:T(8,128)(2,1)} %param.8) | copy-start | bytes 6291460
  2.6 3.9 %copy-start.2 = (bf16[256,4096]{1,0:T(8,128)(2,1)S(1)}, bf16[256,4096]{1,0:T(8,128)(2,1)}, u32[]{:S(2)}) copy-start(bf16[256,4096]{1,0:T(8,128)(2,1)} %param.9) | copy-start | bytes 6291460
  6.5 3.8 %copy-start.5 = (f32[256,2]{0,1:T(2,128)S(1)}, f32[256,2]{0,1:T(2,128)}, u32[]{:S(2)}) copy-start(f32[256,2]{0,1:T(2,128)} %param.12) | copy-start | bytes 6148
  6.5 3.8 %copy-start.7 = (f32[256]{0:T(256)S(1)}, f32[256]{0:T(256)}, u32[]{:S(2)}) copy-start(f32[256]{0:T(256)} %param.11) | copy-start | bytes 3076
  59.1 4.8 %copy-start.1 = (bf16[1,4096,256]{2,1,0:T(8,128)(2,1)S(1)}, bf16[1,4096,256]{2,1,0:T(8,128)(2,1)}, u32[]{:S(2)}) copy-start(bf16[1,4096,256]{2,1,0:T(8,128)(2,1)} %param.14) | copy-start | bytes 6291460
  59.1 5.3 %copy-start.8 = (bf16[4,160,4096]{2,1,0:T(8,128)(2,1)S(1)}, bf16[4,160,4096]{2,1,0:T(8,128)(2,1)}, u32[]{:S(2)}) copy-start(bf16[4,160,4096]{2,1,0:T(8,128)(2,1)} %get-tuple-element.13) | copy-start | bytes 15728644
  64.4 2.4 %copy-start.6 = (f32[4,1,256]{2,1,0:T(1,128)S(1)}, f32[4,1,256]{2,1,0:T(1,128)}, u32[]{:S(2)}) copy-start(f32[4,1,256]{2,1,0:T(1,128)} %get-tuple-element.11) | copy-start | bytes 12292
  71.9 6.1 %copy-start.4 = (bf16[640,256]{1,0:T(8,128)(2,1)}, bf16[640,256]{1,0:T(8,128)(2,1)S(1)}, u32[]{:S(2)}) copy-start(bf16[640,256]{1,0:T(8,128)(2,1)S(1)} %get-tuple-element.19.gu) | copy-start | bytes 983044
  71.9 12.0 %copy-start.3 = (bf16[640,256]{1,0:T(8,128)(2,1)}, bf16[640,256]{1,0:T(8,128)(2,1)S(1)}, u32[]{:S(2)}) copy-start(bf16[640,256]{1,0:T(8,128)(2,1)S(1)} %get-tuple-element.18.gg) | copy-start | bytes 983044
  71.9 12.0 %slice-start = ((s8[5242880]{0:T(1024)(128)(4,1)}), s8[4194304]{0:T(1024)(128)(4,1)S(1)}, s32[]{:S(2)}) async-start(s8[5242880]{0:T(1024)(128)(4,1)} %bitcast.53), calls=%async_computation | async-start | bytes 8388608
  78.0 6.0 %slice-start.1 = ((s8[5242880]{0:T(1024)(128)(4,1)}), s8[1048576]{0:T(1024)(128)(4,1)S(1)}, s32[]{:S(2)}) async-start(s8[5242880]{0:T(1024)(128)(4,1)} %bitcast.53), calls=%async_computation.1 | async-start | bytes 2097152

commit v2 on v1

--- a/solution.py
+++ b/solution.py
@@ -71,8 +71,8 @@
         copy = remote(cs.at[p], c_out.at[ep], c_send.at[d], c_recv.at[d], p, tp)
         copy.start()
         started.append(copy)
-    for a, (src, dst) in enumerate(pairs):
-        for kind, part in ((0, mine), (1, shared)):
+    for kind, part in ((0, mine), (1, shared)):
+        for a, (src, dst) in enumerate(pairs):
             for d, p in enumerate(peers):
                 copy = remote(
                     src.at[p, :, part], dst.at[ep, :, part],
@@ -95,8 +95,8 @@
         stores.append(store)
 
     forwards = []
-    for a, (src, dst) in enumerate(pairs):
-        for kind, part in ((0, mine), (1, shared)):
+    for kind, part in ((0, mine), (1, shared)):
+        for a, (src, dst) in enumerate(pairs):
             for d, p in enumerate(peers):
                 direct[a, kind, d].wait_recv()
                 if kind == 0:
@@ -175,20 +175,29 @@
     )(xs, gs, cs)
 
 
-def return_kernel(n_ep, n_tp, gg, gu, wg, wu, pick, sc, out, sc_out,
+def return_kernel(n_ep, n_tp, ggu, wg, wu, pick, hid, weight, sc, x_hbm, g_hbm,
+                  out, sc_out, gate_out, up_out, down_out,
                   first, first_in, second, second_in, third, third_in,
-                  s1, r1, s2, r2, s3, r3, ss, rs, sl):
+                  xv, gv, gate_v, up_v, down_v,
+                  s1, r1, s2, r2, s3, r3, ss, rs, sl, fetch, flush):
     ep, tp = lax.axis_index("ep"), lax.axis_index("tp")
     core = lax.rem(tp, 2)
     z = tp // 2
     nz = n_tp // 2
     sibling = tp + 1 - 2 * core
     width = out.shape[1]
+    units = wg.shape[1]
     cap = second.shape[2]
     peers = [peer_of(ep, d, n_ep) for d in range(1, n_ep)]
     everyone = [(p, tp) for p in peers]
     everyone += [(ep, lax.rem(tp + k, n_tp)) for k in range(1, n_tp)]
     score_to = [(p, lax.rem(tp + k, n_tp)) for p in [ep] + peers for k in range(n_tp)][1:]
+    fetches = [
+        pltpu.make_async_copy(x_hbm, xv, fetch.at[0]),
+        pltpu.make_async_copy(g_hbm, gv, fetch.at[1]),
+    ]
+    for copy in fetches:
+        copy.start()
     barrier(score_to)
 
     sends = []
@@ -203,9 +212,52 @@
         rows = pl.ds(pl.multiple_of(share * width, width), width)
         dims = (((1,), (1,)), ((), ()))
         return lax.dot_general(
-            gg[...], wg[rows, :], dims, preferred_element_type=F32
-        ) + lax.dot_general(gu[...], wu[rows, :], dims, preferred_element_type=F32)
-
+            ggu[:, :units], wg[rows, :], dims, preferred_element_type=F32
+        ) + lax.dot_general(ggu[:, units:], wu[rows, :], dims, preferred_element_type=F32)
+
+    def tile(t):
+        return pl.ds(pl.multiple_of(t * width, width), width)
+
+    def gate_up_tiles(lo, hi):
+        def step(t, carry):
+            both = lax.dot_general(
+                xv[:, tile(t)], ggu[...], (((0,), (0,)), ((), ())), preferred_element_type=F32
+            ).astype(BF16)
+            gate_v[tile(t), :] = both[:, :units]
+            up_v[tile(t), :] = both[:, units:]
+            return carry
+
+        lax.fori_loop(lo, hi, step, 0)
+
+    def early():
+        fetches[0].wait()
+        gate_up_tiles(0, n_tp // 2)
+
+    def middle():
+        gate_up_tiles(n_tp // 2, n_tp)
+        for k, (src, dst) in enumerate(((gate_v, gate_out), (up_v, up_out))):
+            copy = pltpu.make_async_copy(src, dst, flush.at[k])
+            copy.start()
+            flushes.append(copy)
+
+    def late():
+        fetches[1].wait()
+        hidden_t = hid[...].T
+
+        def step(t, carry):
+            scaled = (weight[...] * gv[:, tile(t)].astype(F32)).astype(BF16)
+            down_v[:, tile(t)] = jnp.dot(
+                hidden_t, scaled, preferred_element_type=F32
+            ).astype(BF16)
+            return carry
+
+        lax.fori_loop(0, n_tp, step, 0)
+        copy = pltpu.make_async_copy(down_v, down_out, flush.at[2])
+        copy.start()
+        flushes.append(copy)
+
+    flushes = []
+    work = [early, middle, late]
     order = [lax.rem(z + dz, nz) for dz in range(nz - 1, -1, -1)]
     halves = []
     for i, zz in enumerate(order):
@@ -227,6 +279,8 @@
             moves[i, d] = copy
     last = []
     for i, zz in enumerate(order):
+        for job in work[i:] if i == nz - 1 else work[i : i + 1]:
+            job()
         for d, p in enumerate(peers):
             moves[i, d].wait_recv()
         second_in[i, ep] = second[i, ep]
@@ -249,12 +303,14 @@
     for copy in sends:
         copy.wait()
     own_score.wait()
-
-
-def give_back(n_ep, n_tp, gg, gu, wg, wu, pick, sc):
+    for copy in flushes:
+        copy.wait()
+
+
+def give_back(n_ep, n_tp, ggu, wg, wu, pick, hid, weight, sc, rows_in, cot_rows):
     vmem = pl.BlockSpec(memory_space=pltpu.VMEM)
     any_spec = pl.BlockSpec(memory_space=pl.ANY)
-    rows, nz = gg.shape[0], n_tp // 2
+    rows, nz = ggu.shape[0], n_tp // 2
     width = wg.shape[0] // n_tp
     tokens = pick.shape[0]
     cap = rows // n_ep
@@ -265,9 +321,12 @@
         out_shape=(
             jax.ShapeDtypeStruct((tokens, width), BF16),
             jax.ShapeDtypeStruct((n_ep, n_tp) + sc.shape[1:], F32),
-        ),
-        in_specs=[vmem] * 5 + [any_spec],
-        out_specs=(vmem, any_spec),
+            jax.ShapeDtypeStruct(wg.shape, BF16),
+            jax.ShapeDtypeStruct(wu.shape, BF16),
+            jax.ShapeDtypeStruct(wg.shape[::-1], BF16),
+        ),
+        in_specs=[vmem] * 6 + [any_spec] * 3,
+        out_specs=(vmem,) + (any_spec,) * 4,
         scratch_shapes=[
             pltpu.VMEM((nz, rows, width), BF16),
             pltpu.VMEM((nz, rows, width), BF16),
@@ -275,16 +334,23 @@
             pltpu.VMEM((nz, n_ep, cap, width), BF16),
             pltpu.VMEM((nz, tokens, width), BF16),
             pltpu.VMEM((nz, tokens, width), BF16),
+            pltpu.VMEM(rows_in.shape, BF16),
+            pltpu.VMEM(cot_rows.shape, BF16),
+            pltpu.VMEM(wg.shape, BF16),
+            pltpu.VMEM(wu.shape, BF16),
+            pltpu.VMEM(wg.shape[::-1], BF16),
             dma((nz,)), dma((nz,)),
             dma((nz, n_ep - 1)), dma((nz, n_ep - 1)),
             dma((nz,)), dma((nz,)),
             dma((others,)), dma((others,)),
             dma,
+            dma((2,)),
+            dma((3,)),
         ],
         compiler_params=pltpu.CompilerParams(
             collective_id=1, has_side_effects=True, vmem_limit_bytes=56 * 1024 * 1024
         ),
-    )(gg, gu, wg, wu, pick, sc)
+    )(ggu, wg, wu, pick, hid, weight, sc, rows_in, cot_rows)
 
 
 def per_device(tokens, cotangent, routing, group_gate, inner_gate, w_gate, w_up, w_down):
@@ -333,10 +399,6 @@
     sigmoid_gate = jax.nn.sigmoid(gate_pre)
     silu_gate = gate_pre * sigmoid_gate
     hidden = (silu_gate * up_pre).astype(BF16)
-    scaled_cot = (row_weight[:, None] * cot_rows).astype(BF16)
-    down_grad = lax.dot_general(
-        hidden, scaled_cot, (((0,), (0,)), ((), ())), preferred_element_type=F32
-    )
     grad_hidden = lax.dot_general(
         cot_rows, down_weight, (((1,), (1,)), ((), ())), preferred_element_type=F32
     )
@@ -346,17 +408,13 @@
         weighted * up_pre * sigmoid_gate * (1.0 + gate_pre * (1.0 - sigmoid_gate))
     ).astype(BF16)
     grad_up_in = (weighted * silu_gate).astype(BF16)
-    gate_grad = lax.dot_general(
-        rows_in, grad_gate_in, (((0,), (0,)), ((), ())), preferred_element_type=F32
-    )
-    upper_grad = lax.dot_general(
-        rows_in, grad_up_in, (((0,), (0,)), ((), ())), preferred_element_type=F32
-    )
     send_score = jnp.pad(
         partial_scores.reshape(n_ep, 1, cap), ((0, 0), (0, 0), (0, pad))
     )
-    token_grad, all_scores = give_back(
-        n_ep, n_tp, grad_gate_in, grad_up_in, gate_weight, up_weight, put.T, send_score
+    token_grad, all_scores, gate_grad, upper_grad, down_grad = give_back(
+        n_ep, n_tp, jnp.concatenate([grad_gate_in, grad_up_in], axis=1),
+        gate_weight, up_weight, put.T, hidden, row_weight[:, None], send_score,
+        rows_in, cot_rows,
     )
     scores = jnp.sum(all_scores[:, :, 0, :cap], axis=1).reshape(rows)
     score_t = jnp.sum(jnp.where(hits, scores[:, None, None], 0.0), axis=0)
@@ -367,9 +425,9 @@
         token_grad,
         group_grad,
         inner_grad,
-        gate_grad.astype(BF16)[None],
-        upper_grad.astype(BF16)[None],
-        down_grad.astype(BF16)[None],
+        gate_grad[None],
+        upper_grad[None],
+        down_grad[None],
     )
 
 

time: 139 us -> 132 us (0.950)
  matrix products: 35.3 us -> 20.7 us
  local copies, waits for them, and re-layouts: 3.99 us -> 11.8 us
  Pallas kernels: 93.5 us -> 92.1 us
    dot_general x3 -> x0, matrix products: 15.2 us -> none  [the longest x1 6.03 us: per_device(): lax.dot_general(hidden, scaled_cot, (((0,), (0,)), ((), ())), preferred_e...]
    unnamed x23 -> x22, local copies, waits for them, and re-layouts: 2.15 us -> 9.03 us
    pallas_call x1, Pallas kernels: 47.9 us -> 46.1 us  [dispatch(): pl.pallas_call(functools.partial(dispatch_kernel, n_ep, n_tp), out_shape=...]
where the time goes in v2:
time: 132 us; the launch traced here: 131 us
  Pallas kernels  92.1 us (70%)
  matrix products  20.7 us (16%)
  local copies, waits for them, and re-layouts  11.8 us (9%)
  other arithmetic  5.85 us (4%)
    pallas_call x1, Pallas kernels, dispatch(): pl.pallas_call(functools.partial(dispatch_kernel, n_ep, n_tp), out_shape=...  46.1 us
    pallas_call x1, Pallas kernels, give_back(): pl.pallas_call(functools.partial(return_kernel, n_ep, n_tp), out_shape=(j...  46 us
    unnamed x22, local copies, waits for them, and re-layouts  9.03 us
    dot_general x2, matrix products, placed(): jnp.dot(put, source, preferred_element_type=F32).astype(BF16)  7.68 us
    dot_general x1, matrix products, per_device(): lax.dot_general(cot_rows, down_weight, (((1,), (1,)), ((), ())), preferre...  5.72 us
    dot_general x1, matrix products, per_device(): gate_pre = jnp.dot(rows_in, gate_weight, preferred_element_type=F32)  4.81 us

profile of v2, /device:TPU:0, one launch (start us, length us, event | category | flops | bytes accessed | tf_op | source)
XLA Modules:
  0.0 131.2 jit_solution(11678975112914654358)
XLA Ops:
  0.6 0.0 copy-start
  0.6 0.8 convert_reduce_fusion
  1.5 0.1 fusion.3
  1.6 0.7 select_reduce_fusion.2
  2.4 0.2 fusion.2
  2.6 3.9 %convolution_convert_fusion.1 = bf16[640,4096]{1,0:T(8,128)(2,1)} fusion(pred[640,256]{1,0:T(8,128)(4,1)S(1)} %fusion.2, bf16[256,4096]{1,0:T(8,128)(2,1)S(1)} %copy-done), kind=kOutput, calls=%fused_computation.1 | convolution fusion | flops 1344798720 | bytes 7503872 | tf_op jit(solution)/shard_map/dot_general | solution.py:385
  6.5 3.8 %convolution_convert_fusion = bf16[640,4096]{1,0:T(8,128)(2,1)} fusion(pred[640,256]{1,0:T(8,128)(4,1)S(1)} %fusion.2, bf16[256,4096]{1,0:T(8,128)(2,1)S(1)} %copy-done.5), kind=kOutput, calls=%fused_computation | convolution fusion | flops 1344798720 | bytes 7503872 | tf_op jit(solution)/shard_map/dot_general | solution.py:385
  10.3 0.2 select_reduce_fusion.1
  10.5 0.1 reshape.47
  10.6 0.6 pad.7.cs
  11.2 46.1 %shard_map.127 = (bf16[4,160,4096]{2,1,0:T(8,128)(2,1)}, bf16[4,160,4096]{2,1,0:T(8,128)(2,1)}, f32[4,1,256]{2,1,0:T(1,128)}) custom-call(bf16[4,160,4096]{2,1,0:T(8,128)(2,1)} %bitcast.36, bf16[4,160,4096]{2,1,0:T(8,128)(2,1)} %bitcast.37, f32[4,1,256]{2,1,0:T(1,128)} %pad.7.cs), custom_call_target="tpu_custom_call" | custom-call | tf_op jit(solution)/shard_map/pallas_call | solution.py:157
  57.3 4.8 %fusion.7 = f32[640,256]{1,0:T(8,128)S(1)} fusion(bf16[640,4096]{1,0:T(8,128)(2,1)} %bitcast.38, bf16[1,4096,256]{2,1,0:T(8,128)(2,1)} %param.13), kind=kOutput, calls=%fused_computation.30 | convolution fusion | flops 1342177280 | bytes 7995392 | tf_op jit(solution)/shard_map/dot_general | solution.py:397
  62.1 0.5 copy-done.2
  62.6 2.4 %fusion.9 = f32[640,256]{1,0:T(8,128)} fusion(bf16[640,4096]{1,0:T(8,128)(2,1)S(1)} %bitcast.40, bf16[1,4096,256]{2,1,0:T(8,128)(2,1)S(1)} %copy-done.2), kind=kOutput, calls=%fused_computation.32 | convolution fusion | flops 1342177280 | bytes 7995392 | tf_op jit(solution)/shard_map/dot_general | solution.py:398
  65.0 0.1 mul.62
  65.0 5.7 %multiply_reduce_fusion = (f32[640]{0:T(1024)S(1)}, bf16[640,256]{1,0:T(8,128)(2,1)}, bf16[640,256]{1,0:T(8,128)(2,1)S(1)}, bf16[640,256]{1,0:T(8,128)(2,1)S(1)}) fusion(f32[640,256]{1,0:T(8,128)} %fusion.9, f32[640,256]{1,0:T(8,128)S(1)} %fusion.7, f32[640]{0:T(1024)S(1)} %mul.62, bf16[640,4096]{1,0:T(8,128)(2,1)} %bitcast.41, bf16[1,256,4096]{2,1,0:T(8,128)(2,1)} %param.15), kind=kOutput, calls=%fused_computation.11 | convolution fusion | flops 1345289600 | bytes 9638912 | tf_op jit(solution)/shard_map/dot_general | solution.py:402
  70.8 0.9 pad_maximum_fusion.ggu
  71.7 0.1 reshape.50
  71.7 0.6 pad.8.sc
  72.3 1.0 broadcast_in_dim_reshape_squeeze.5.weight
  73.3 0.3 copy.34
  73.6 0.8 convert_bitcast_fusion.pick
  74.3 46.0 %shard_map.128 = (bf16[256,512]{1,0:T(8,128)(2,1)}, f32[4,8,1,256]{3,2,1,0:T(1,128)}, bf16[4096,256]{1,0:T(8,128)(2,1)}, bf16[4096,256]{1,0:T(8,128)(2,1)}, bf16[256,4096]{1,0:T(8,128)(2,1)}) custom-call(bf16[640,512]{1,0:T(8,128)(2,1)} %pad_maximum_fusion.ggu, bf16[4096,256]{1,0:T(8,128)(2,1)} %bitcast.44, bf16[4096,256]{1,0:T(8,128)(2,1)} %bitcast.43, ...), custom_call_target="tpu_custom_call" | custom-call | tf_op jit(solution)/shard_map/pallas_call | solution.py:319
  120.4 0.8 slice_reduce_fusion
  121.2 0.1 broadcast_in_dim.62
  121.2 0.3 select_reduce_fusion
  121.5 1.1 bitcast_multiply_fusion
  122.6 1.7 %copy.45 = bf16[256,512]{1,0:T(8,128)(2,1)} copy(bf16[256,512]{1,0:T(8,128)(2,1)} %get-tuple-element.34) | data formatting | bytes 524288
  124.3 3.2 %copy.46 = bf16[1,4096,256]{2,1,0:T(8,128)(2,1)} copy(bf16[1,4096,256]{2,1,0:T(8,128)(2,1)} %bitcast.47) | data formatting | bytes 4194304
  127.5 1.3 %copy.47 = bf16[1,4096,256]{2,1,0:T(8,128)(2,1)} copy(bf16[1,4096,256]{2,1,0:T(8,128)(2,1)S(1)} %bitcast.46) | data formatting | bytes 4194304
  128.8 1.0 copy-done.3
  129.9 1.3 %copy.48 = bf16[1,256,4096]{2,1,0:T(8,128)(2,1)} copy(bf16[1,256,4096]{2,1,0:T(8,128)(2,1)S(1)} %bitcast.45) | data formatting | bytes 4194304
  (18 shorter events, 0.1 us)
Async XLA Ops:
  0.6 2.0 %copy-start = (bf16[256,4096]{1,0:T(8,128)(2,1)S(1)}, bf16[256,4096]{1,0:T(8,128)(2,1)}, u32[]{:S(2)}) copy-start(bf16[256,4096]{1,0:T(8,128)(2,1)} %param.8) | copy-start | bytes 6291460
  2.6 3.9 %copy-start.5 = (bf16[256,4096]{1,0:T(8,128)(2,1)S(1)}, bf16[256,4096]{1,0:T(8,128)(2,1)}, u32[]{:S(2)}) copy-start(bf16[256,4096]{1,0:T(8,128)(2,1)} %param.9) | copy-start | bytes 6291460
  6.5 3.8 %copy-start.6 = (f32[256,2]{0,1:T(2,128)S(1)}, f32[256,2]{0,1:T(2,128)}, u32[]{:S(2)}) copy-start(f32[256,2]{0,1:T(2,128)} %param.12) | copy-start | bytes 6148
  6.5 3.8 %copy-start.8 = (f32[256]{0:T(256)S(1)}, f32[256]{0:T(256)}, u32[]{:S(2)}) copy-start(f32[256]{0:T(256)} %param.11) | copy-start | bytes 3076
  57.3 4.8 %copy-start.1 = (bf16[4,160,4096]{2,1,0:T(8,128)(2,1)S(1)}, bf16[4,160,4096]{2,1,0:T(8,128)(2,1)}, u32[]{:S(2)}) copy-start(bf16[4,160,4096]{2,1,0:T(8,128)(2,1)} %get-tuple-element.16) | copy-start | bytes 15728644
  57.3 5.3 %copy-start.2 = (bf16[1,4096,256]{2,1,0:T(8,128)(2,1)S(1)}, bf16[1,4096,256]{2,1,0:T(8,128)(2,1)}, u32[]{:S(2)}) copy-start(bf16[1,4096,256]{2,1,0:T(8,128)(2,1)} %param.14) | copy-start | bytes 6291460
  62.6 2.4 %copy-start.7 = (f32[4,1,256]{2,1,0:T(1,128)S(1)}, f32[4,1,256]{2,1,0:T(1,128)}, u32[]{:S(2)}) copy-start(f32[4,1,256]{2,1,0:T(1,128)} %get-tuple-element.14) | copy-start | bytes 12292
  124.3 3.2 %copy-start.4 = (bf16[4096,256]{1,0:T(8,128)(2,1)S(1)}, bf16[4096,256]{1,0:T(8,128)(2,1)}, u32[]{:S(2)}) copy-start(bf16[4096,256]{1,0:T(8,128)(2,1)} %get-tuple-element.20) | copy-start | bytes 6291460
  127.5 2.3 %copy-start.3 = (bf16[256,4096]{1,0:T(8,128)(2,1)S(1)}, bf16[256,4096]{1,0:T(8,128)(2,1)}, u32[]{:S(2)}) copy-start(bf16[256,4096]{1,0:T(8,128)(2,1)} %get-tuple-element.21) | copy-start | bytes 6291460

commit v3 on v2

--- a/solution.py
+++ b/solution.py
@@ -23,13 +23,13 @@
     return out
 
 
-def barrier(partners):
+def greet(partners):
     sem = pltpu.get_barrier_semaphore()
     for ep, tp in partners:
         pl.semaphore_signal(
             sem, inc=1, device_id=(ep, tp), device_id_type=pl.DeviceIdType.MESH
         )
-    pl.semaphore_wait(sem, len(partners))
+    return lambda: pl.semaphore_wait(sem, len(partners))
 
 
 def remote(src, dst, send, recv, ep, tp):
@@ -56,7 +56,7 @@
     both = half - 2 * lone
     base = core * half
     peers = [peer_of(ep, d, n_ep) for d in range(1, n_ep)]
-    barrier([(p, tp) for p in peers] + [(ep, sibling), (ep, across)])
+    greet([(p, tp) for p in peers] + [(ep, sibling), (ep, across)])()
 
     def cols(start, width):
         return pl.ds(pl.multiple_of(start, LANES), width)
@@ -175,11 +175,11 @@
     )(xs, gs, cs)
 
 
-def return_kernel(n_ep, n_tp, ggu, wg, wu, pick, hid, weight, sc, x_hbm, g_hbm,
+def return_kernel(n_ep, n_tp, ggu, pick, hid, weight, sc, x_hbm, g_hbm, wg_hbm, wu_hbm,
                   out, sc_out, gate_out, up_out, down_out,
                   first, first_in, second, second_in, third, third_in,
-                  xv, gv, gate_v, up_v, down_v,
-                  s1, r1, s2, r2, s3, r3, ss, rs, sl, fetch, flush):
+                  xv, gv, gate_v, up_v, down_v, wg, wu,
+                  s1, r1, s2, r2, s3, r3, ss, rs, sl, fetch, flush, w_sem):
     ep, tp = lax.axis_index("ep"), lax.axis_index("tp")
     core = lax.rem(tp, 2)
     z = tp // 2
@@ -189,24 +189,22 @@
     units = wg.shape[1]
     cap = second.shape[2]
     peers = [peer_of(ep, d, n_ep) for d in range(1, n_ep)]
-    everyone = [(p, tp) for p in peers]
-    everyone += [(ep, lax.rem(tp + k, n_tp)) for k in range(1, n_tp)]
     score_to = [(p, lax.rem(tp + k, n_tp)) for p in [ep] + peers for k in range(n_tp)][1:]
+    order = [lax.rem(z + dz, nz) for dz in range(nz - 1, -1, -1)]
+    weight_fetches = []
+    for i, zz in enumerate(order):
+        rows = pl.ds(pl.multiple_of(2 * zz * width, width), 2 * width)
+        for k, (src, dst) in enumerate(((wg_hbm, wg), (wu_hbm, wu))):
+            copy = pltpu.make_async_copy(src.at[rows], dst.at[rows], w_sem.at[k, i])
+            copy.start()
+            weight_fetches.append(copy)
     fetches = [
         pltpu.make_async_copy(x_hbm, xv, fetch.at[0]),
         pltpu.make_async_copy(g_hbm, gv, fetch.at[1]),
     ]
     for copy in fetches:
         copy.start()
-    barrier(score_to)
-
-    sends = []
-    for i, (p, t) in enumerate(score_to):
-        copy = remote(sc.at[p], sc_out.at[ep, tp], ss.at[i], rs.at[i], p, t)
-        copy.start()
-        sends.append(copy)
-    own_score = pltpu.make_async_copy(sc.at[ep], sc_out.at[ep, tp], sl)
-    own_score.start()
+    arrived = greet(score_to)
 
     def partial(share):
         rows = pl.ds(pl.multiple_of(share * width, width), width)
@@ -258,13 +256,31 @@
 
     flushes = []
     work = [early, middle, late]
-    order = [lax.rem(z + dz, nz) for dz in range(nz - 1, -1, -1)]
     halves = []
-    for i, zz in enumerate(order):
-        first[i] = partial(2 * zz + 1 - core).astype(BF16)
+
+    def prepare(i):
+        for copy in weight_fetches[2 * i : 2 * i + 2]:
+            copy.wait()
+        first[i] = partial(2 * order[i] + 1 - core).astype(BF16)
+
+    def push(i):
         copy = remote(first.at[i], first_in.at[i], s1.at[i], r1.at[i], ep, sibling)
         copy.start()
         halves.append(copy)
+
+    ahead = min(2, nz)
+    for i in range(ahead):
+        prepare(i)
+    arrived()
+    for i in range(ahead):
+        push(i)
+    sends = []
+    for i, (p, t) in enumerate(score_to):
+        copy = remote(sc.at[p], sc_out.at[ep, tp], ss.at[i], rs.at[i], p, t)
+        copy.start()
+        sends.append(copy)
+    own_score = pltpu.make_async_copy(sc.at[ep], sc_out.at[ep, tp], sl)
+    own_score.start()
     moves = {}
     for i, zz in enumerate(order):
         total = partial(2 * zz + core)
@@ -277,6 +293,9 @@
             )
             copy.start()
             moves[i, d] = copy
+        if i + ahead < nz:
+            prepare(i + ahead)
+            push(i + ahead)
     last = []
     for i, zz in enumerate(order):
         for job in work[i:] if i == nz - 1 else work[i : i + 1]:
@@ -325,7 +344,7 @@
             jax.ShapeDtypeStruct(wu.shape, BF16),
             jax.ShapeDtypeStruct(wg.shape[::-1], BF16),
         ),
-        in_specs=[vmem] * 6 + [any_spec] * 3,
+        in_specs=[vmem] * 4 + [any_spec] * 5,
         out_specs=(vmem,) + (any_spec,) * 4,
         scratch_shapes=[
             pltpu.VMEM((nz, rows, width), BF16),
@@ -339,6 +358,8 @@
             pltpu.VMEM(wg.shape, BF16),
             pltpu.VMEM(wu.shape, BF16),
             pltpu.VMEM(wg.shape[::-1], BF16),
+            pltpu.VMEM(wg.shape, BF16),
+            pltpu.VMEM(wu.shape, BF16),
             dma((nz,)), dma((nz,)),
             dma((nz, n_ep - 1)), dma((nz, n_ep - 1)),
             dma((nz,)), dma((nz,)),
@@ -346,11 +367,12 @@
             dma,
             dma((2,)),
             dma((3,)),
+            dma((2, nz)),
         ],
         compiler_params=pltpu.CompilerParams(
             collective_id=1, has_side_effects=True, vmem_limit_bytes=56 * 1024 * 1024
         ),
-    )(ggu, wg, wu, pick, hid, weight, sc, rows_in, cot_rows)
+    )(ggu, pick, hid, weight, sc, rows_in, cot_rows, wg, wu)
 
 
 def per_device(tokens, cotangent, routing, group_gate, inner_gate, w_gate, w_up, w_down):

time: 132 us -> 133 us (level)
  Pallas kernels: 92.1 us -> 93.5 us
    pallas_call x1, Pallas kernels: 46 us -> 47.5 us  [give_back(): pl.pallas_call(functools.partial(return_kernel, n_ep, n_tp), out_shape=(j...]
where the time goes in v3:
time: 133 us
  Pallas kernels  93.5 us (70%)
  matrix products  20.7 us (16%)
  local copies, waits for them, and re-layouts  11.8 us (9%)
  other arithmetic  5.85 us (4%)
    pallas_call x1, Pallas kernels, give_back(): pl.pallas_call(functools.partial(return_kernel, n_ep, n_tp), out_shape=(j...  47.5 us
    pallas_call x1, Pallas kernels, dispatch(): pl.pallas_call(functools.partial(dispatch_kernel, n_ep, n_tp), out_shape=...  46.1 us
    unnamed x22, local copies, waits for them, and re-layouts  9.03 us
    dot_general x2, matrix products, placed(): jnp.dot(put, source, preferred_element_type=F32).astype(BF16)  7.68 us
    dot_general x1, matrix products, per_device(): lax.dot_general(cot_rows, down_weight, (((1,), (1,)), ((), ())), preferre...  5.72 us
    dot_general x1, matrix products, per_device(): gate_pre = jnp.dot(rows_in, gate_weight, preferred_element_type=F32)  4.81 us

profile of v3, /device:TPU:0, one launch (start us, length us, event | category | flops | bytes accessed | tf_op | source)
XLA Modules:
  0.0 132.6 jit_solution(4743831545894667773)
XLA Ops:
  0.6 0.0 copy-start
  0.6 0.8 convert_reduce_fusion
  1.5 0.1 fusion.3
  1.6 0.7 select_reduce_fusion.2
  2.4 0.2 fusion.2
  2.6 3.9 %convolution_convert_fusion.1 = bf16[640,4096]{1,0:T(8,128)(2,1)} fusion(pred[640,256]{1,0:T(8,128)(4,1)S(1)} %fusion.2, bf16[256,4096]{1,0:T(8,128)(2,1)S(1)} %copy-done), kind=kOutput, calls=%fused_computation.1 | convolution fusion | flops 1344798720 | bytes 7503872 | tf_op jit(solution)/shard_map/dot_general | solution.py:407
  6.5 3.8 %convolution_convert_fusion = bf16[640,4096]{1,0:T(8,128)(2,1)} fusion(pred[640,256]{1,0:T(8,128)(4,1)S(1)} %fusion.2, bf16[256,4096]{1,0:T(8,128)(2,1)S(1)} %copy-done.5), kind=kOutput, calls=%fused_computation | convolution fusion | flops 1344798720 | bytes 7503872 | tf_op jit(solution)/shard_map/dot_general | solution.py:407
  10.3 0.2 select_reduce_fusion.1
  10.5 0.1 reshape.47
  10.6 0.6 pad.7.cs
  11.2 46.1 %shard_map.127 = (bf16[4,160,4096]{2,1,0:T(8,128)(2,1)}, bf16[4,160,4096]{2,1,0:T(8,128)(2,1)}, f32[4,1,256]{2,1,0:T(1,128)}) custom-call(bf16[4,160,4096]{2,1,0:T(8,128)(2,1)} %bitcast.36, bf16[4,160,4096]{2,1,0:T(8,128)(2,1)} %bitcast.37, f32[4,1,256]{2,1,0:T(1,128)} %pad.7.cs), custom_call_target="tpu_custom_call" | custom-call | tf_op jit(solution)/shard_map/pallas_call | solution.py:157
  57.3 4.8 %fusion.7 = f32[640,256]{1,0:T(8,128)S(1)} fusion(bf16[640,4096]{1,0:T(8,128)(2,1)} %bitcast.38, bf16[1,4096,256]{2,1,0:T(8,128)(2,1)} %param.13), kind=kOutput, calls=%fused_computation.30 | convolution fusion | flops 1342177280 | bytes 7995392 | tf_op jit(solution)/shard_map/dot_general | solution.py:419
  62.1 0.5 copy-done.2
  62.6 2.4 %fusion.9 = f32[640,256]{1,0:T(8,128)} fusion(bf16[640,4096]{1,0:T(8,128)(2,1)S(1)} %bitcast.40, bf16[1,4096,256]{2,1,0:T(8,128)(2,1)S(1)} %copy-done.2), kind=kOutput, calls=%fused_computation.32 | convolution fusion | flops 1342177280 | bytes 7995392 | tf_op jit(solution)/shard_map/dot_general | solution.py:420
  65.0 0.1 mul.62
  65.0 5.7 %multiply_reduce_fusion = (f32[640]{0:T(1024)S(1)}, bf16[640,256]{1,0:T(8,128)(2,1)}, bf16[640,256]{1,0:T(8,128)(2,1)S(1)}, bf16[640,256]{1,0:T(8,128)(2,1)S(1)}) fusion(f32[640,256]{1,0:T(8,128)} %fusion.9, f32[640,256]{1,0:T(8,128)S(1)} %fusion.7, f32[640]{0:T(1024)S(1)} %mul.62, bf16[640,4096]{1,0:T(8,128)(2,1)} %bitcast.41, bf16[1,256,4096]{2,1,0:T(8,128)(2,1)} %param.15), kind=kOutput, calls=%fused_computation.11 | convolution fusion | flops 1345289600 | bytes 9638912 | tf_op jit(solution)/shard_map/dot_general | solution.py:424
  70.8 0.9 pad_maximum_fusion.ggu
  71.7 0.1 reshape.50
  71.7 0.6 pad.8.sc
  72.3 1.0 broadcast_in_dim_reshape_squeeze.5.weight
  73.3 0.3 copy.34
  73.6 0.8 convert_bitcast_fusion.pick
  74.3 47.5 %shard_map.128 = (bf16[256,512]{1,0:T(8,128)(2,1)}, f32[4,8,1,256]{3,2,1,0:T(1,128)}, bf16[4096,256]{1,0:T(8,128)(2,1)}, bf16[4096,256]{1,0:T(8,128)(2,1)}, bf16[256,4096]{1,0:T(8,128)(2,1)}) custom-call(bf16[640,512]{1,0:T(8,128)(2,1)} %pad_maximum_fusion.ggu, bf16[256,640]{1,0:T(8,128)(2,1)} %convert_bitcast_fusion.pick, ...), custom_call_target="tpu_custom_call" | custom-call | tf_op jit(solution)/shard_map/pallas_call | solution.py:338
  121.8 0.8 slice_reduce_fusion
  122.6 0.1 broadcast_in_dim.62
  122.7 0.3 select_reduce_fusion
  123.0 1.1 bitcast_multiply_fusion
  124.1 1.7 %copy.45 = bf16[256,512]{1,0:T(8,128)(2,1)} copy(bf16[256,512]{1,0:T(8,128)(2,1)} %get-tuple-element.34) | data formatting | bytes 524288
  125.8 3.2 %copy.46 = bf16[1,4096,256]{2,1,0:T(8,128)(2,1)} copy(bf16[1,4096,256]{2,1,0:T(8,128)(2,1)} %bitcast.47) | data formatting | bytes 4194304
  129.0 1.3 copy.47
  130.3 1.0 copy-done.3
  131.3 1.3 copy.48
  (18 shorter events, 0.1 us)
Async XLA Ops:
  0.6 2.0 %copy-start = (bf16[256,4096]{1,0:T(8,128)(2,1)S(1)}, bf16[256,4096]{1,0:T(8,128)(2,1)}, u32[]{:S(2)}) copy-start(bf16[256,4096]{1,0:T(8,128)(2,1)} %param.8) | copy-start | bytes 6291460
  2.6 3.9 %copy-start.5 = (bf16[256,4096]{1,0:T(8,128)(2,1)S(1)}, bf16[256,4096]{1,0:T(8,128)(2,1)}, u32[]{:S(2)}) copy-start(bf16[256,4096]{1,0:T(8,128)(2,1)} %param.9) | copy-start | bytes 6291460
  6.5 3.8 %copy-start.6 = (f32[256,2]{0,1:T(2,128)S(1)}, f32[256,2]{0,1:T(2,128)}, u32[]{:S(2)}) copy-start(f32[256,2]{0,1:T(2,128)} %param.12) | copy-start | bytes 6148
  6.5 3.8 %copy-start.8 = (f32[256]{0:T(256)S(1)}, f32[256]{0:T(256)}, u32[]{:S(2)}) copy-start(f32[256]{0:T(256)} %param.11) | copy-start | bytes 3076
  57.3 4.8 %copy-start.1 = (bf16[4,160,4096]{2,1,0:T(8,128)(2,1)S(1)}, bf16[4,160,4096]{2,1,0:T(8,128)(2,1)}, u32[]{:S(2)}) copy-start(bf16[4,160,4096]{2,1,0:T(8,128)(2,1)} %get-tuple-element.16) | copy-start | bytes 15728644
  57.3 5.3 %copy-start.2 = (bf16[1,4096,256]{2,1,0:T(8,128)(2,1)S(1)}, bf16[1,4096,256]{2,1,0:T(8,128)(2,1)}, u32[]{:S(2)}) copy-start(bf16[1,4096,256]{2,1,0:T(8,128)(2,1)} %param.14) | copy-start | bytes 6291460
  62.6 2.4 %copy-start.7 = (f32[4,1,256]{2,1,0:T(1,128)S(1)}, f32[4,1,256]{2,1,0:T(1,128)}, u32[]{:S(2)}) copy-start(f32[4,1,256]{2,1,0:T(1,128)} %get-tuple-element.14) | copy-start | bytes 12292
  125.8 3.2 %copy-start.4 = (bf16[4096,256]{1,0:T(8,128)(2,1)S(1)}, bf16[4096,256]{1,0:T(8,128)(2,1)}, u32[]{:S(2)}) copy-start(bf16[4096,256]{1,0:T(8,128)(2,1)} %get-tuple-element.20) | copy-start | bytes 6291460
  129.0 2.3 %copy-start.3 = (bf16[256,4096]{1,0:T(8,128)(2,1)S(1)}, bf16[256,4096]{1,0:T(8,128)(2,1)}, u32[]{:S(2)}) copy-start(bf16[256,4096]{1,0:T(8,128)(2,1)} %get-tuple-element.21) | copy-start | bytes 6291460
